TPU v7x, 32 devices: a whole 2x2x4 slice. The times are simulated.
32 devices in a mesh: grp: 2 (over x), ep: 16 (over z, y, core).
Axes of the slice: x: 2, y: 2, z: 4, core: 2. Of those that a mesh axis runs over, the one named last changes fastest.
Arguments:
- resid: bfloat16 [384, 2048], P(('grp', 'ep')), parts along dimension 0, may hold values from -6 to 6
- norm_gains: float32 [4, 2048], replicated, may hold values from 0.1 to 1.9
- w_query: bfloat16 [2048, 1024], P(None, 'ep'), may hold values from -0.125 to 0.125
- w_key: bfloat16 [2048, 1024], P(None, 'ep'), may hold values from -0.125 to 0.125
- w_value: bfloat16 [2048, 1024], P(None, 'ep'), may hold values from -0.125 to 0.125
- w_outgate: bfloat16 [2048, 1024], P(None, 'ep'), may hold values from -0.125 to 0.125
- w_igate: bfloat16 [2048, 8], replicated, may hold values from -0.125 to 0.125
- w_fgate: bfloat16 [2048, 8], replicated, may hold values from -0.125 to 0.125
- igate_bias: float32 [8], replicated, may hold values from -1 to 1
- fgate_bias: float32 [8], replicated, may hold values from -1 to 5
- state_matrix: float32 [384, 8, 128, 128], P(('grp', 'ep')), parts along dimension 0, may hold values from -0.8 to 0.8
- state_norm: float32 [384, 8, 128], P(('grp', 'ep')), parts along dimension 0, may hold values from -2.4 to 2.4
- state_max: float32 [384, 8], P(('grp', 'ep')), parts along dimension 0, may hold values from -1 to 1
- w_mix_out: bfloat16 [1024, 2048], replicated, may hold values from -0.1875 to 0.1875
- routes: int32 [384, 2], P(('grp', 'ep')), parts along dimension 0, may hold values from 0 to 15, all different within a row; in each aligned block of 12 rows (0 to 11, 12 to 23, ...) at most 2 rows name the same one
- route_scores: bfloat16 [384, 2], P(('grp', 'ep')), parts along dimension 0, may hold values from 0.099609375 to 1
- expert_gate: bfloat16 [16, 2048, 512], P('ep'), may hold values from -0.125 to 0.125
- expert_up: bfloat16 [16, 2048, 512], P('ep'), may hold values from -0.125 to 0.125
- expert_down: bfloat16 [16, 512, 2048], P('ep'), may hold values from -0.25 to 0.25
- dense_gate: bfloat16 [2048, 8192], P(None, 'ep'), may hold values from -0.125 to 0.125
- dense_up: bfloat16 [2048, 8192], P(None, 'ep'), may hold values from -0.125 to 0.125
- dense_down: bfloat16 [8192, 2048], P('ep'), may hold values from -0.0625 to 0.0625
- branch_weight: bfloat16 [2048], replicated, may hold values from -0.125 to 0.125
Outputs:
- out_stream: bfloat16 [384, 2048], P(('grp', 'ep')), parts along dimension 0
- new_matrix: float32 [384, 8, 128, 128], P(('grp', 'ep')), parts along dimension 0
- new_norm: float32 [384, 8, 128], P(('grp', 'ep')), parts along dimension 0
- new_max: float32 [384, 8], P(('grp', 'ep')), parts along dimension 0
There are 2 independent parts, one for each index of `grp`. A program takes and returns all parts, laid end to end along the dimension named above; an argument that names none is the same for every part. Nothing has to cross between parts.
Inputs may be any that keep to these rules, and one draw needn't show every extreme that they name: `routes`: each row names 2 different experts. In each aligned block of 12 rows (the rows of one device) no expert is named by more than 2 rows, a bound that some block reaches.
All inputs are finite; a program needn't handle non-finite values.
Results may differ from a plain program's by a relative error of at most 0.015.
Values may be sent and summed in bfloat16 or wider, within the bound.
A program may use at most 128 MiB of HBM per device.

v0:
```python
import jax
import jax.numpy as jnp
from jax import lax
from jax.sharding import PartitionSpec as P

CAP = 2


def rms_scale(values, gains):
    return values * lax.rsqrt(jnp.mean(values * values, axis=-1, keepdims=True) + 1e-06) * gains


def expert_batch(picked, gate_matrix, up_matrix, down_matrix):
    gate_out = jnp.einsum("jrd,jdf->jrf", picked, gate_matrix, preferred_element_type=jnp.float32)
    up_out = jnp.einsum("jrd,jdf->jrf", picked, up_matrix, preferred_element_type=jnp.float32)
    hidden = (jax.nn.silu(gate_out) * up_out).astype(jnp.bfloat16)
    return jnp.einsum(
        "jrf,jfd->jrd", hidden, down_matrix, preferred_element_type=jnp.float32
    ).astype(jnp.bfloat16)


def route_tables(routes, route_scores, expert_ids):
    onehot = (routes[:, :, None] == expert_ids[None, None, :]).astype(jnp.float32)
    scores = route_scores.astype(jnp.float32)
    shares = scores / jnp.sum(scores, axis=-1, keepdims=True)
    weights = jnp.sum(shares[:, :, None] * onehot, axis=1)
    hit_count = jnp.sum(onehot, axis=1)
    return (weights, hit_count)


def exchanged_experts(
    branch_in, routes, route_scores, expert_gate, expert_up, expert_down, devices_ep
):
    experts = expert_gate.shape[0] * devices_ep
    weights, hit_count = route_tables(routes, route_scores, jnp.arange(experts, dtype=jnp.int32))
    hit_int = hit_count.astype(jnp.int32)
    rank_index = jnp.cumsum(hit_int, axis=0) - hit_int
    slot_range = jnp.arange(CAP, dtype=jnp.int32)
    chosen = (
        (rank_index.T[:, None, :] == slot_range[None, :, None]) & (hit_count.T[:, None, :] > 0.5)
    ).astype(jnp.float32)
    outgoing = jnp.einsum(
        "ect,td->ecd", chosen.astype(jnp.bfloat16), branch_in, preferred_element_type=jnp.float32
    ).astype(jnp.bfloat16)
    incoming = lax.all_to_all(outgoing, "ep", split_axis=0, concat_axis=1, tiled=True)
    produced = expert_batch(incoming, expert_gate, expert_up, expert_down)
    returned = lax.all_to_all(produced, "ep", split_axis=1, concat_axis=0, tiled=True)
    weighted = chosen * weights.T[:, None, :]
    each_expert = jnp.einsum(
        "ect,ecd->etd", weighted, returned.astype(jnp.float32), precision=lax.Precision.HIGHEST
    )
    return jnp.sum(each_expert.astype(jnp.bfloat16).astype(jnp.float32), axis=0)


def local(
    resid,
    norm_gains,
    w_query,
    w_key,
    w_value,
    w_outgate,
    w_igate,
    w_fgate,
    igate_bias,
    fgate_bias,
    state_matrix,
    state_norm,
    state_max,
    w_mix_out,
    routes,
    route_scores,
    expert_gate,
    expert_up,
    expert_down,
    dense_gate,
    dense_up,
    dense_down,
    branch_weight,
):
    seqs_local = resid.shape[0]
    heads = state_matrix.shape[1]
    head_size = state_matrix.shape[2]
    devices_ep = lax.axis_size("ep")
    resid32 = resid.astype(jnp.float32)
    normed = rms_scale(resid32, norm_gains[0]).astype(jnp.bfloat16)
    row_piece = lax.all_gather(normed, "ep", axis=0, tiled=True)
    projected = jnp.stack(
        [
            jnp.dot(row_piece, matrix, preferred_element_type=jnp.float32).astype(jnp.bfloat16)
            for matrix in (w_query, w_key, w_value, w_outgate)
        ],
        axis=1,
    )
    own_proj = lax.all_to_all(projected, "ep", split_axis=0, concat_axis=2, tiled=True)
    head_shape = (seqs_local, heads, head_size)
    query = own_proj[:, 0].astype(jnp.float32).reshape(head_shape)
    key_heads = own_proj[:, 1].astype(jnp.float32).reshape(head_shape) * head_size ** (-0.5)
    value_heads = own_proj[:, 2].astype(jnp.float32).reshape(head_shape)
    outgate = own_proj[:, 3].astype(jnp.float32).reshape(head_shape)
    ipre = jnp.dot(normed, w_igate, preferred_element_type=jnp.float32) + igate_bias
    fpre = jnp.dot(normed, w_fgate, preferred_element_type=jnp.float32) + fgate_bias
    logf = jax.nn.log_sigmoid(fpre)
    new_max = jnp.maximum(ipre, logf + state_max)
    keep_gain = jnp.exp(logf + state_max - new_max)
    write_gain = jnp.exp(ipre - new_max)
    new_matrix = (
        keep_gain[:, :, None, None] * state_matrix
        + write_gain[:, :, None, None] * value_heads[:, :, :, None] * key_heads[:, :, None, :]
    )
    new_norm = keep_gain[:, :, None] * state_norm + write_gain[:, :, None] * key_heads
    numer = jnp.einsum("shed,shd->she", new_matrix, query, precision=lax.Precision.HIGHEST)
    denom = jnp.sum(new_norm * query, axis=-1)
    cell = numer / jnp.maximum(jnp.abs(denom), 1.0)[:, :, None]
    gated = (
        (jax.nn.sigmoid(outgate) * cell).reshape(seqs_local, heads * head_size).astype(jnp.bfloat16)
    )
    mixed = jnp.dot(gated, w_mix_out, preferred_element_type=jnp.float32)
    middle = resid32 + rms_scale(mixed, norm_gains[1])
    branch_in = rms_scale(middle, norm_gains[2]).astype(jnp.bfloat16)
    all_rows = lax.all_gather(branch_in, "ep", axis=0, tiled=True)
    moe_own = exchanged_experts(
        branch_in, routes, route_scores, expert_gate, expert_up, expert_down, devices_ep
    )
    gate_out = jnp.dot(all_rows, dense_gate, preferred_element_type=jnp.float32)
    up_out = jnp.dot(all_rows, dense_up, preferred_element_type=jnp.float32)
    hidden = (jax.nn.silu(gate_out) * up_out).astype(jnp.bfloat16)
    logit = jnp.dot(all_rows, branch_weight, preferred_element_type=jnp.float32)
    summed = lax.psum_scatter(
        (
            jnp.dot(hidden, dense_down, preferred_element_type=jnp.float32)
            * jax.nn.sigmoid(logit)[:, None]
        ).astype(jnp.bfloat16),
        "ep",
        scatter_dimension=0,
        tiled=True,
    ).astype(jnp.float32)
    combined = moe_own + summed
    out_stream = (middle + rms_scale(combined, norm_gains[3])).astype(jnp.bfloat16)
    return (out_stream, new_matrix, new_norm, new_max)


def solution(mesh):
    placed = (
        P(("grp", "ep"), None),
        P(),
        P(None, "ep"),
        P(None, "ep"),
        P(None, "ep"),
        P(None, "ep"),
        P(),
        P(),
        P(),
        P(),
        P(("grp", "ep"), None, None, None),
        P(("grp", "ep"), None, None),
        P(("grp", "ep"), None),
        P(),
        P(("grp", "ep"), None),
        P(("grp", "ep"), None),
        P("ep", None, None),
        P("ep", None, None),
        P("ep", None, None),
        P(None, "ep"),
        P(None, "ep"),
        P("ep", None),
        P(),
    )
    return jax.shard_map(
        local,
        mesh=mesh,
        in_specs=placed,
        out_specs=(
            P(("grp", "ep"), None),
            P(("grp", "ep"), None, None, None),
            P(("grp", "ep"), None, None),
            P(("grp", "ep"), None),
        ),
        check_vma=False,
    )
```

profile of v0, /device:TPU:17, one launch (start us, length us, event | category | flops | bytes accessed | tf_op | source)
XLA Modules:
  0.0 161.0 jit_solution(14762901746730829710)
XLA Ops:
  0.7 1.0 fusion.62
  3.6 21.5 %all-gather = bf16[16,12,2048]{2,1,0:T(8,128)(2,1)} all-gather(bf16[1,12,2048]{2,1,0:T(8,128)(2,1)S(1)} %fusion.61), channel_id=1, replica_groups=mesh['grp'=2,'ep'=16] {'ep'}, dimensions={0}, use_global_device_ids=true | all-gather | bytes 835584 | tf_op jit(solution)/shard_map/all_gather | solution.py:86
  25.1 1.3 reshape.139
  29.2 8.6 %all-to-all-start = ((bf16[16,2,1536]{2,1,0:T(2,128)(2,1)}), bf16[16,2,1536]{2,1,0:T(2,128)(2,1)S(1)}, u32[]{:S(2)}, u32[]{:S(2)}) async-start(bf16[16,2,1536]{2,1,0:T(2,128)(2,1)} %reshape.151), calls=%async_computation | async-start | bytes 196608 | tf_op jit(solution)/shard_map/all_to_all | solution.py:94
  39.2 3.3 %all-to-all-done = bf16[16,2,1536]{2,1,0:T(2,128)(2,1)S(1)} async-done(((bf16[16,2,1536]{2,1,0:T(2,128)(2,1)}), bf16[16,2,1536]{2,1,0:T(2,128)(2,1)S(1)}, u32[]{:S(2)}, u32[]{:S(2)}) %all-to-all-start) | async-done | bytes 98336 | tf_op jit(solution)/shard_map/all_to_all | solution.py:94
  44.0 4.5 %multiply_add_fusion = f32[12,8,128,128]{3,2,1,0:T(8,128)S(1)} fusion(f32[12,8,128,128]{3,2,1,0:T(8,128)} %param.33, f32[12,8,128]{2,1,0:T(8,128)S(1)} %get-tuple-element.14, f32[12,8,128]{2,1,0:T(8,128)S(1)} %get-tuple-element.21, f32[12,8]{1,0:T(8,128)S(1)} %copy.78), kind=kLoop, calls=%fused_computation | loop fusion | flops 4718592 | bytes 12681600 | tf_op jit(solution)/shard_map/add | solution.py:107
  48.5 5.0 %fusion.43 = f32[12,8,1,128]{3,2,1,0:T(1,128)S(1)} fusion(f32[12,8,128,128]{3,2,1,0:T(8,128)S(1)} %multiply_add_fusion, bf16[12,4,1024]{2,1,0:T(4,128)(2,1)S(1)} %all_to_all.32), kind=kOutput, calls=%fused_computation.61 | convolution fusion | flops 18874368 | bytes 6389760 | tf_op jit(solution)/shard_map/shed,shd->she/dot_general | solution.py:111
  54.8 22.2 %all-gather.1 = bf16[16,12,2048]{2,1,0:T(8,128)(2,1)} all-gather(bf16[1,12,2048]{2,1,0:T(8,128)(2,1)S(1)} %fusion.58), channel_id=1, replica_groups=mesh['grp'=2,'ep'=16] {'ep'}, dimensions={0}, use_global_device_ids=true | all-gather | bytes 835584 | tf_op jit(solution)/shard_map/all_gather | solution.py:120
  77.0 1.3 reshape.141
  78.3 2.9 %fusion.63 = f32[192,512]{1,0:T(8,128)} fusion(bf16[192,2048]{1,0:T(8,128)(2,1)S(1)} %reshape.141, bf16[2048,512]{1,0:T(8,128)(2,1)} %param.42), kind=kOutput, calls=%fused_computation.106 | convolution fusion | flops 402653184 | bytes 3276800 | tf_op jit(solution)/shard_map/dot_general | solution.py:124
  82.6 6.1 %all-to-all-start.1 = ((bf16[16,2,2048]{2,1,0:T(2,128)(2,1)}), bf16[16,2,2048]{2,1,0:T(2,128)(2,1)S(1)}, u32[]{:S(2)}, u32[]{:S(2)}) async-start(bf16[16,2,2048]{2,1,0:T(2,128)(2,1)} %copy.88), calls=%async_computation.1 | async-start | bytes 262144 | tf_op jit(solution)/shard_map/all_to_all | solution.py:45
  88.7 3.6 %fusion.2 = bf16[192,2048]{1,0:T(8,128)(2,1)} fusion(bf16[512,2048]{1,0:T(8,128)(2,1)S(1)} %copy-done, bf16[192,2048]{1,0:T(8,128)(2,1)S(1)} %reshape.141, bf16[2048,512]{1,0:T(8,128)(2,1)} %param.43, f32[192]{0:T(256)S(1)} %add_divide_fusion, f32[192,512]{1,0:T(8,128)} %fusion.63), kind=kOutput, calls=%fused_computation.4 | convolution fusion | flops 806682624 | bytes 6161152 | tf_op jit(solution)/shard_map/dot_general | solution.py:130
  92.3 1.8 %all-to-all-done.1 = bf16[16,2,2048]{2,1,0:T(2,128)(2,1)S(1)} async-done(((bf16[16,2,2048]{2,1,0:T(2,128)(2,1)}), bf16[16,2,2048]{2,1,0:T(2,128)(2,1)S(1)}, u32[]{:S(2)}, u32[]{:S(2)}) %all-to-all-start.1) | async-done | bytes 131104 | tf_op jit(solution)/shard_map/all_to_all | solution.py:45
  94.2 2.0 %fusion.7 = f32[32,512]{1,0:T(8,128)S(1)} fusion(bf16[32,2048]{1,0:T(8,128)(2,1)S(1)} %reshape.130, bf16[1,2048,512]{2,1,0:T(8,128)(2,1)} %param.39), kind=kOutput, calls=%fused_computation.11 | convolution fusion | flops 67108864 | bytes 2293760 | tf_op jit(solution)/shard_map/jrd,jdf->jrf/dot_general | solution.py:14
  96.2 3.2 %fusion.3 = bf16[1,32,2048]{2,1,0:T(8,128)(2,1)S(1)} fusion(bf16[1,512,2048]{2,1,0:T(8,128)(2,1)} %param.41, bf16[32,2048]{1,0:T(8,128)(2,1)S(1)} %reshape.130, bf16[1,2048,512]{2,1,0:T(8,128)(2,1)} %param.40, f32[32,512]{1,0:T(8,128)S(1)} %fusion.7), kind=kOutput, calls=%fused_computation.7 | convolution fusion | flops 134381568 | bytes 4521984 | tf_op jit(solution)/shard_map/jrf,jfd->jrd/dot_general | solution.py:17
  100.2 1.4 reduce.4
  102.3 6.0 %all-to-all-start.2 = ((bf16[16,2,2048]{2,1,0:T(2,128)(2,1)}), bf16[16,2,2048]{2,1,0:T(2,128)(2,1)S(1)}, u32[]{:S(2)}, u32[]{:S(2)}) async-start(bf16[16,2,2048]{2,1,0:T(2,128)(2,1)} %reshape.153), calls=%async_computation.2 | async-start | bytes 262144 | tf_op jit(solution)/shard_map/all_to_all | solution.py:47
  108.3 28.7 %fusion = bf16[16,2048]{1,0:T(8,128)(2,1)S(1)} fusion(bf16[192,2048]{1,0:T(8,128)(2,1)S(1)} %copy-done.4), kind=kCustom, calls=%all-reduce-scatter | all-reduce-scatter fusion | flops 524289 | bytes 852480
  137.0 2.6 %collective-permute-start = (bf16[16,2048]{1,0:T(8,128)(2,1)S(1)}, bf16[16,2048]{1,0:T(8,128)(2,1)S(1)}, u32[]{:S(2)}, u32[]{:S(2)}) collective-permute-start(bf16[16,2048]{1,0:T(8,128)(2,1)S(1)} %fusion), channel_id=1, source_target_pairs={{0,1},{1,2},{2,3},{3,4},{4,5},{5,6},{6,7},{7,8},{8,9},{9,10},{10,1... | collective-permute-start | bytes 196616
  139.6 5.4 %collective-permute-start.1 = (bf16[16,2048]{1,0:T(8,128)(2,1)S(1)}, bf16[16,2048]{1,0:T(8,128)(2,1)S(1)}, u32[]{:S(2)}, u32[]{:S(2)}) collective-permute-start(bf16[16,2048]{1,0:T(8,128)(2,1)S(1)} %fusion), channel_id=1, source_target_pairs={{0,2},{1,3},{2,4},{3,5},{4,6},{5,7},{6,8},{7,9},{8,10},{9,11},{10,... | collective-permute-start | bytes 196616
  145.0 7.3 %collective-permute-start.2 = (bf16[16,2048]{1,0:T(8,128)(2,1)S(1)}, bf16[16,2048]{1,0:T(8,128)(2,1)S(1)}, u32[]{:S(2)}, u32[]{:S(2)}) collective-permute-start(bf16[16,2048]{1,0:T(8,128)(2,1)S(1)} %fusion), channel_id=1, source_target_pairs={{0,3},{1,4},{2,5},{3,6},{4,7},{5,8},{6,9},{7,10},{8,11},{9,12},{10... | collective-permute-start | bytes 196616
  152.3 1.9 %collective-permute-start.3 = (bf16[12,2048]{1,0:T(8,128)(2,1)S(1)}, bf16[12,2048]{1,0:T(8,128)(2,1)S(1)}, u32[]{:S(2)}, u32[]{:S(2)}) collective-permute-start(bf16[12,2048]{1,0:T(8,128)(2,1)S(1)} %slice.36), channel_id=1, source_target_pairs={{0,4},{1,5},{2,6},{3,7},{4,8},{5,9},{6,10},{7,11},{8,12},{9,13},{1... | collective-permute-start | bytes 147464
  155.6 1.8 %collective-permute-done.3 = bf16[12,2048]{1,0:T(8,128)(2,1)S(1)} collective-permute-done((bf16[12,2048]{1,0:T(8,128)(2,1)S(1)}, bf16[12,2048]{1,0:T(8,128)(2,1)S(1)}, u32[]{:S(2)}, u32[]{:S(2)}) %collective-permute-start.3) | collective-permute-done | bytes 49184
  159.1 1.1 fusion.9
  (107 shorter events, 14.8 us)
Async XLA Ops:
  0.6 88.1 %copy-start = (bf16[512,2048]{1,0:T(8,128)(2,1)S(1)}, bf16[512,2048]{1,0:T(8,128)(2,1)}, u32[]{:S(2)}) copy-start(bf16[512,2048]{1,0:T(8,128)(2,1)} %param.44) | copy-start | bytes 6291460
  0.6 25.8 %copy-start.5 = (bf16[2048,64]{0,1:T(8,128)(2,1)S(1)}, bf16[2048,64]{0,1:T(8,128)(2,1)}, u32[]{:S(2)}) copy-start(bf16[2048,64]{0,1:T(8,128)(2,1)} %param.25) | copy-start | bytes 786436
  2.6 24.2 %copy-start.6 = (bf16[2048,64]{0,1:T(8,128)(2,1)S(1)}, bf16[2048,64]{0,1:T(8,128)(2,1)}, u32[]{:S(2)}) copy-start(bf16[2048,64]{0,1:T(8,128)(2,1)} %param.26) | copy-start | bytes 786436
  26.8 10.9 %copy-start.14 = (bf16[12,2]{0,1:T(2,128)(2,1)S(1)}, bf16[12,2]{0,1:T(2,128)(2,1)}, u32[]{:S(2)}) copy-start(bf16[12,2]{0,1:T(2,128)(2,1)} %param.38) | copy-start | bytes 148
  26.9 11.1 %copy-start.12 = (s32[12,2]{0,1:T(2,128)S(1)}, s32[12,2]{0,1:T(2,128)}, u32[]{:S(2)}) copy-start(s32[12,2]{0,1:T(2,128)} %param.37) | copy-start | bytes 292
  26.9 11.3 %copy-start.3 = (bf16[12,2048]{1,0:T(8,128)(2,1)S(1)}, bf16[12,2048]{1,0:T(8,128)(2,1)}, u32[]{:S(2)}) copy-start(bf16[12,2048]{1,0:T(8,128)(2,1)} %param.23) | copy-start | bytes 147460
  26.9 11.3 %copy-start.15 = (bf16[2048,8]{0,1:T(8,128)(2,1)S(1)}, bf16[2048,8]{0,1:T(8,128)(2,1)}, u32[]{:S(2)}) copy-start(bf16[2048,8]{0,1:T(8,128)(2,1)} %param.30) | copy-start | bytes 98308
  26.9 11.3 %copy-start.17 = (f32[12,8]{0,1:T(8,128)S(1)}, f32[12,8]{0,1:T(8,128)}, u32[]{:S(2)}) copy-start(f32[12,8]{0,1:T(8,128)} %param.35) | copy-start | bytes 1156
  26.9 11.3 %copy-start.18 = (f32[8]{0:T(128)S(1)}, f32[8]{0:T(128)}, u32[]{:S(2)}) copy-start(f32[8]{0:T(128)} %param.32) | copy-start | bytes 100
  26.9 11.5 %copy-start.16 = (bf16[2048,8]{0,1:T(8,128)(2,1)S(1)}, bf16[2048,8]{0,1:T(8,128)(2,1)}, u32[]{:S(2)}) copy-start(bf16[2048,8]{0,1:T(8,128)(2,1)} %param.29) | copy-start | bytes 98308
  26.9 11.5 %copy-start.19 = (f32[8]{0:T(128)S(1)}, f32[8]{0:T(128)}, u32[]{:S(2)}) copy-start(f32[8]{0:T(128)} %param.31) | copy-start | bytes 100
  27.4 11.5 %copy-start.10 = (bf16[2048]{0:T(1024)(128)(2,1)S(1)}, bf16[2048]{0:T(1024)(128)(2,1)}, u32[]{:S(2)}) copy-start(bf16[2048]{0:T(1024)(128)(2,1)} %param.45) | copy-start | bytes 12292
  27.8 15.5 %copy-start.9 = (f32[12,8,128]{2,1,0:T(8,128)S(1)}, f32[12,8,128]{2,1,0:T(8,128)}, u32[]{:S(2)}) copy-start(f32[12,8,128]{2,1,0:T(8,128)} %param.34) | copy-start | bytes 147460
  29.2 13.3 %all-to-all-start = ((bf16[16,2,1536]{2,1,0:T(2,128)(2,1)}), bf16[16,2,1536]{2,1,0:T(2,128)(2,1)S(1)}, u32[]{:S(2)}, u32[]{:S(2)}) async-start(bf16[16,2,1536]{2,1,0:T(2,128)(2,1)} %reshape.151), calls=%async_computation | async-start | bytes 196608 | tf_op jit(solution)/shard_map/all_to_all | solution.py:94
  38.6 9.8 %copy-start.11 = (f32[12,8]{0,1:T(8,128)}, f32[12,8]{0,1:T(8,128)S(1)}, u32[]{:S(2)}) copy-start(f32[12,8]{0,1:T(8,128)S(1)} %get-tuple-element.10) | copy-start | bytes 1156
  48.5 5.1 %copy-start.2 = (bf16[1024,2048]{1,0:T(8,128)(2,1)S(1)}, bf16[1024,2048]{1,0:T(8,128)(2,1)}, u32[]{:S(2)}) copy-start(bf16[1024,2048]{1,0:T(8,128)(2,1)} %param.36) | copy-start | bytes 12582916
  82.6 11.5 %all-to-all-start.1 = ((bf16[16,2,2048]{2,1,0:T(2,128)(2,1)}), bf16[16,2,2048]{2,1,0:T(2,128)(2,1)S(1)}, u32[]{:S(2)}, u32[]{:S(2)}) async-start(bf16[16,2,2048]{2,1,0:T(2,128)(2,1)} %copy.88), calls=%async_computation.1 | async-start | bytes 262144 | tf_op jit(solution)/shard_map/all_to_all | solution.py:45
  96.2 12.1 %copy-start.4 = (bf16[192,2048]{1,0:T(8,128)(2,1)S(1)}, bf16[192,2048]{1,0:T(8,128)(2,1)}, u32[]{:S(2)}) copy-start(bf16[192,2048]{1,0:T(8,128)(2,1)} %fusion.2) | copy-start | bytes 2359300
  99.4 54.9 %copy-start.13 = (u32[32]{0:T(128)S(1)}, u32[32]{0:T(128)}, u32[]{:S(2)}) copy-start(u32[32]{0:T(128)} %constant.42) | copy-start | bytes 388
  102.3 55.8 %all-to-all-start.2 = ((bf16[16,2,2048]{2,1,0:T(2,128)(2,1)}), bf16[16,2,2048]{2,1,0:T(2,128)(2,1)S(1)}, u32[]{:S(2)}, u32[]{:S(2)}) async-start(bf16[16,2,2048]{2,1,0:T(2,128)(2,1)} %reshape.153), calls=%async_computation.2 | async-start | bytes 262144 | tf_op jit(solution)/shard_map/all_to_all | solution.py:47
  137.0 20.4 %collective-permute-start = (bf16[16,2048]{1,0:T(8,128)(2,1)S(1)}, bf16[16,2048]{1,0:T(8,128)(2,1)S(1)}, u32[]{:S(2)}, u32[]{:S(2)}) collective-permute-start(bf16[16,2048]{1,0:T(8,128)(2,1)S(1)} %fusion), channel_id=1, source_target_pairs={{0,1},{1,2},{2,3},{3,4},{4,5},{5,6},{6,7},{7,8},{8,9},{9,10},{10,1... | collective-permute-start | bytes 196616
  139.6 17.7 %collective-permute-start.1 = (bf16[16,2048]{1,0:T(8,128)(2,1)S(1)}, bf16[16,2048]{1,0:T(8,128)(2,1)S(1)}, u32[]{:S(2)}, u32[]{:S(2)}) collective-permute-start(bf16[16,2048]{1,0:T(8,128)(2,1)S(1)} %fusion), channel_id=1, source_target_pairs={{0,2},{1,3},{2,4},{3,5},{4,6},{5,7},{6,8},{7,9},{8,10},{9,11},{10,... | collective-permute-start | bytes 196616
  145.0 12.3 %collective-permute-start.2 = (bf16[16,2048]{1,0:T(8,128)(2,1)S(1)}, bf16[16,2048]{1,0:T(8,128)(2,1)S(1)}, u32[]{:S(2)}, u32[]{:S(2)}) collective-permute-start(bf16[16,2048]{1,0:T(8,128)(2,1)S(1)} %fusion), channel_id=1, source_target_pairs={{0,3},{1,4},{2,5},{3,6},{4,7},{5,8},{6,9},{7,10},{8,11},{9,12},{10... | collective-permute-start | bytes 196616
  152.3 5.0 %collective-permute-start.3 = (bf16[12,2048]{1,0:T(8,128)(2,1)S(1)}, bf16[12,2048]{1,0:T(8,128)(2,1)S(1)}, u32[]{:S(2)}, u32[]{:S(2)}) collective-permute-start(bf16[12,2048]{1,0:T(8,128)(2,1)S(1)} %slice.36), channel_id=1, source_target_pairs={{0,4},{1,5},{2,6},{3,7},{4,8},{5,9},{6,10},{7,11},{8,12},{9,13},{1... | collective-permute-start | bytes 147464
  (3 other events, 7.3 us)
where the time goes:
time: 162 us; the launch traced here: 161 us
  blocking collectives  72.4 us (45%)
  starting transfers between devices  37.8 us (23%)
  matrix products  21.1 us (13%)
  local copies, waits for them, and re-layouts  10.5 us (6%)
  other arithmetic  10.4 us (6%)
  waiting for transfers between devices  6.9 us (4%)
  between operations  1.84 us (1%)
    unnamed x1, blocking collectives  28.7 us
    all_gather x1, blocking collectives, local(): all_rows = lax.all_gather(branch_in, 'ep', axis=0, tiled=True)  22.2 us
    all_gather x1, blocking collectives, local(): row_piece = lax.all_gather(normed, 'ep', axis=0, tiled=True)  21.5 us
    unnamed x4, starting transfers between devices  17.2 us
    all_to_all x1, starting transfers between devices, local(): lax.all_to_all(projected, 'ep', split_axis=0, concat_axis=2, tiled=True)  8.56 us
    unnamed x55, local copies, waits for them, and re-layouts  6.65 us
    all_to_all x1, starting transfers between devices, exchanged_experts(): lax.all_to_all(outgoing, 'ep', split_axis=0, concat_axis=1, tiled=True)  6.08 us
    all_to_all x1, starting transfers between devices, exchanged_experts(): lax.all_to_all(produced, 'ep', split_axis=1, concat_axis=0, tiled=True)  5.97 us
  transfers between devices with their start and end apart: 7, of which 3 were waited for; matrix products, arithmetic and copies ran while one was open for 22% of the time, Pallas kernels for 0%

commit v1 on v0

--- a/solution.py
+++ b/solution.py
@@ -117,7 +117,13 @@
     mixed = jnp.dot(gated, w_mix_out, preferred_element_type=jnp.float32)
     middle = resid32 + rms_scale(mixed, norm_gains[1])
     branch_in = rms_scale(middle, norm_gains[2]).astype(jnp.bfloat16)
-    all_rows = lax.all_gather(branch_in, "ep", axis=0, tiled=True)
+    count = lax.axis_size("ep")
+    held, pieces = (branch_in, [branch_in])
+    for _ in range(count - 1):
+        held = lax.ppermute(held, "ep", [(i, (i + 1) % count) for i in range(count)])
+        pieces.insert(0, held)
+    line = jnp.concatenate(pieces, axis=0)
+    all_rows = jnp.roll(line, (lax.axis_index("ep") + 1) * branch_in.shape[0], axis=0)
     moe_own = exchanged_experts(
         branch_in, routes, route_scores, expert_gate, expert_up, expert_down, devices_ep
     )

time: 162 us -> 254 us (1.57)
  starting transfers between devices: 37.8 us -> 85.9 us
  local copies, waits for them, and re-layouts: 10.5 us -> 51.7 us
  waiting for transfers between devices: 6.9 us -> 26.3 us
  blocking collectives: 72.4 us -> 54.1 us
    concatenate x0 -> x1, local copies, waits for them, and re-layouts: none -> 37.9 us  [local(): jnp.roll(line, (lax.axis_index('ep') + 1) * branch_in.shape[0], axis=0)]
    ppermute x0 -> x15, starting transfers between devices: none -> 25.1 us  [local(): lax.ppermute(held, 'ep', [(i, (i + 1) % count) for i in range(count)])]
    all_gather x1 -> x0, blocking collectives: 22.2 us -> none  [local(): all_rows = lax.all_gather(branch_in, 'ep', axis=0, tiled=True)]
    ppermute x0 -> x15, waiting for transfers between devices: none -> 21.3 us  [local(): lax.ppermute(held, 'ep', [(i, (i + 1) % count) for i in range(count)])]
    all_to_all x1, starting transfers between devices: 5.97 us -> 16.7 us  [exchanged_experts(): lax.all_to_all(produced, 'ep', split_axis=1, concat_axis=0, tiled=True)]
    all_to_all x1, starting transfers between devices: 6.08 us -> 13.3 us  [exchanged_experts(): lax.all_to_all(outgoing, 'ep', split_axis=0, concat_axis=1, tiled=True)]
    unnamed x4, starting transfers between devices: 17.2 us -> 22.2 us
    unnamed x1, blocking collectives: 28.7 us -> 32.6 us
  transfers between devices with their start and end apart: 7 -> 22, of which waited for: 3 -> 13; matrix products, arithmetic and copies ran while one was open for 22% -> 6% of each run, Pallas kernels for 0% -> 0%
where the time goes in v1:
time: 254 us; the launch traced here: 252 us
  starting transfers between devices  85.9 us (34%)
  blocking collectives  54.1 us (21%)
  local copies, waits for them, and re-layouts  51.7 us (20%)
  waiting for transfers between devices  26.3 us (10%)
  matrix products  20.9 us (8%)
  other arithmetic  11.1 us (4%)
    concatenate x1, local copies, waits for them, and re-layouts, local(): jnp.roll(line, (lax.axis_index('ep') + 1) * branch_in.shape[0], axis=0)  37.9 us
    unnamed x1, blocking collectives  32.6 us
    ppermute x15, starting transfers between devices, local(): lax.ppermute(held, 'ep', [(i, (i + 1) % count) for i in range(count)])  25.1 us
    unnamed x4, starting transfers between devices  22.2 us
    all_gather x1, blocking collectives, local(): row_piece = lax.all_gather(normed, 'ep', axis=0, tiled=True)  21.5 us
    ppermute x15, waiting for transfers between devices, local(): lax.ppermute(held, 'ep', [(i, (i + 1) % count) for i in range(count)])  21.3 us
    all_to_all x1, starting transfers between devices, exchanged_experts(): lax.all_to_all(produced, 'ep', split_axis=1, concat_axis=0, tiled=True)  16.7 us
    all_to_all x1, starting transfers between devices, exchanged_experts(): lax.all_to_all(outgoing, 'ep', split_axis=0, concat_axis=1, tiled=True)  13.3 us
  transfers between devices with their start and end apart: 22, of which 13 were waited for; matrix products, arithmetic and copies ran while one was open for 6% of the time, Pallas kernels for 0%

profile of v1, /device:TPU:17, one launch (start us, length us, event | category | flops | bytes accessed | tf_op | source)
XLA Modules:
  0.0 251.8 jit_solution(8267765139773000615)
XLA Ops:
  4.2 21.5 %all-gather = bf16[16,12,2048]{2,1,0:T(8,128)(2,1)} all-gather(bf16[1,12,2048]{2,1,0:T(8,128)(2,1)S(1)} %fusion.68), channel_id=1, replica_groups=mesh['grp'=2,'ep'=16] {'ep'}, dimensions={0}, use_global_device_ids=true | all-gather | bytes 835584 | tf_op jit(solution)/shard_map/all_gather | solution.py:86
  29.8 8.6 %all-to-all-start = ((bf16[16,2,1536]{2,1,0:T(2,128)(2,1)}), bf16[16,2,1536]{2,1,0:T(2,128)(2,1)S(1)}, u32[]{:S(2)}, u32[]{:S(2)}) async-start(bf16[16,2,1536]{2,1,0:T(2,128)(2,1)} %reshape.149), calls=%async_computation | async-start | bytes 196608 | tf_op jit(solution)/shard_map/all_to_all | solution.py:94
  40.8 2.3 all-to-all-done
  44.6 4.5 %multiply_add_fusion = f32[12,8,128,128]{3,2,1,0:T(8,128)S(1)} fusion(f32[12,8,128,128]{3,2,1,0:T(8,128)} %param.33, f32[12,8,128]{2,1,0:T(8,128)S(1)} %get-tuple-element.14, f32[12,8,128]{2,1,0:T(8,128)S(1)} %get-tuple-element.21, f32[12,8]{1,0:T(8,128)S(1)} %copy.78), kind=kLoop, calls=%fused_computation | loop fusion | flops 4718592 | bytes 12681600 | tf_op jit(solution)/shard_map/add | solution.py:107
  49.1 5.0 %fusion.47 = f32[12,8,1,128]{3,2,1,0:T(1,128)S(1)} fusion(f32[12,8,128,128]{3,2,1,0:T(8,128)S(1)} %multiply_add_fusion, bf16[12,4,1024]{2,1,0:T(4,128)(2,1)S(1)} %all_to_all.32), kind=kOutput, calls=%fused_computation.61 | convolution fusion | flops 18874368 | bytes 6389760 | tf_op jit(solution)/shard_map/shed,shd->she/dot_general | solution.py:111
  57.3 2.4 collective-permute-start.1
  64.2 13.3 %all-to-all-start.1 = ((bf16[16,2,2048]{2,1,0:T(2,128)(2,1)}), bf16[16,2,2048]{2,1,0:T(2,128)(2,1)S(1)}, u32[]{:S(2)}, u32[]{:S(2)}) async-start(bf16[16,2,2048]{2,1,0:T(2,128)(2,1)} %copy.88), calls=%async_computation.1 | async-start | bytes 262144 | tf_op jit(solution)/shard_map/all_to_all | solution.py:45
  80.5 2.8 %collective-permute-start.4 = (bf16[12,2048]{1,0:T(8,128)(2,1)S(1)}, bf16[12,2048]{1,0:T(8,128)(2,1)S(1)}, u32[]{:S(2)}, u32[]{:S(2)}) collective-permute-start(bf16[12,2048]{1,0:T(8,128)(2,1)S(1)} %collective-permute-done.3), channel_id=1, source_target_pairs={{0,1},{1,2},{2,3},{3,4},{4,5},{5,6},{6,7},{7,8},{8,9},{9,10},{10,1... | collective-permute-start | bytes 147464 | tf_op jit(solution)/shard_map/ppermute | solution.py:123
  87.0 2.5 collective-permute-done.5
  90.7 3.3 %collective-permute-done.6 = bf16[12,2048]{1,0:T(8,128)(2,1)S(1)} collective-permute-done((bf16[12,2048]{1,0:T(8,128)(2,1)S(1)}, bf16[12,2048]{1,0:T(8,128)(2,1)S(1)}, u32[]{:S(2)}, u32[]{:S(2)}) %collective-permute-start.6) | collective-permute-done | bytes 49184 | tf_op jit(solution)/shard_map/ppermute | solution.py:123
  96.4 2.3 collective-permute-done.7
  98.6 3.1 %fusion.3 = bf16[1,32,2048]{2,1,0:T(8,128)(2,1)S(1)} fusion(bf16[1,512,2048]{2,1,0:T(8,128)(2,1)} %param.41, bf16[32,2048]{1,0:T(8,128)(2,1)S(1)} %reshape.130, bf16[1,2048,512]{2,1,0:T(8,128)(2,1)} %param.40, f32[32,512]{1,0:T(8,128)S(1)} %fusion.7), kind=kOutput, calls=%fused_computation.7 | convolution fusion | flops 134381568 | bytes 4521984 | tf_op jit(solution)/shard_map/jrf,jfd->jrd/dot_general | solution.py:17
  104.0 3.2 %collective-permute-start.9 = (bf16[12,2048]{1,0:T(8,128)(2,1)S(1)}, bf16[12,2048]{1,0:T(8,128)(2,1)S(1)}, u32[]{:S(2)}, u32[]{:S(2)}) collective-permute-start(bf16[12,2048]{1,0:T(8,128)(2,1)S(1)} %collective-permute-done.8), channel_id=1, source_target_pairs={{0,1},{1,2},{2,3},{3,4},{4,5},{5,6},{6,7},{7,8},{8,9},{9,10},{10,1... | collective-permute-start | bytes 147464 | tf_op jit(solution)/shard_map/ppermute | solution.py:123
  107.9 16.7 %all-to-all-start.2 = ((bf16[16,2,2048]{2,1,0:T(2,128)(2,1)}), bf16[16,2,2048]{2,1,0:T(2,128)(2,1)S(1)}, u32[]{:S(2)}, u32[]{:S(2)}) async-start(bf16[16,2,2048]{2,1,0:T(2,128)(2,1)} %reshape.151), calls=%async_computation.2 | async-start | bytes 262144 | tf_op jit(solution)/shard_map/all_to_all | solution.py:47
  127.6 2.8 %collective-permute-start.11 = (bf16[12,2048]{1,0:T(8,128)(2,1)S(1)}, bf16[12,2048]{1,0:T(8,128)(2,1)S(1)}, u32[]{:S(2)}, u32[]{:S(2)}) collective-permute-start(bf16[12,2048]{1,0:T(8,128)(2,1)S(1)} %collective-permute-done.10), channel_id=1, source_target_pairs={{0,1},{1,2},{2,3},{3,4},{4,5},{5,6},{6,7},{7,8},{8,9},{9,10},{10,1... | collective-permute-start | bytes 147464 | tf_op jit(solution)/shard_map/ppermute | solution.py:123
  134.1 2.6 %collective-permute-done.12 = bf16[12,2048]{1,0:T(8,128)(2,1)} collective-permute-done((bf16[12,2048]{1,0:T(8,128)(2,1)S(1)}, bf16[12,2048]{1,0:T(8,128)(2,1)}, u32[]{:S(2)}, u32[]{:S(2)}) %collective-permute-start.12) | collective-permute-done | bytes 49184 | tf_op jit(solution)/shard_map/ppermute | solution.py:123
  146.5 37.9 %concatenate.6 = bf16[384,2048]{1,0:T(8,128)(2,1)} concatenate(bf16[12,2048]{1,0:T(8,128)(2,1)} %collective-permute-done.14, bf16[12,2048]{1,0:T(8,128)(2,1)} %collective-permute-done.13, bf16[12,2048]{1,0:T(8,128)(2,1)} %collective-permute-done.12, bf16[12,2048]{1,0:T(8,128)(2,1)S(1)} %collective-permute-done.11, bf16[12,2048]{1,0:T(8,128)(2,1)S(1)} %collective-permute-done.10, ...), dimensions={0} | concatenate | bytes 3145728 | tf_op jit(solution)/shard_map/jit(_roll_dynamic)/concatenate | solution.py:126
  184.5 2.5 %fusion.25 = f32[192,512]{1,0:T(8,128)S(1)} fusion(bf16[2048,512]{1,0:T(8,128)(2,1)} %param.43, bf16[384,2048]{1,0:T(8,128)(2,1)} %concatenate.6, s32[]{:T(128)S(6)} %select_n.20), kind=kOutput, calls=%fused_computation.29 | convolution fusion | flops 402653184 | bytes 3276804 | tf_op jit(solution)/shard_map/dot_general | solution.py:131
  187.4 3.9 %fusion.2 = bf16[192,2048]{1,0:T(8,128)(2,1)} fusion(bf16[512,2048]{1,0:T(8,128)(2,1)S(1)} %copy-done, f32[192]{0:T(256)S(1)} %add_divide_fusion, f32[192,512]{1,0:T(8,128)S(1)} %fusion.25, bf16[2048,512]{1,0:T(8,128)(2,1)} %param.42, bf16[384,2048]{1,0:T(8,128)(2,1)} %concatenate.6, s32[]{:T(128)S(6)} %select_n.20), kind=kOutput, calls=%fused_computation.4 | convolution fusion | flops 806682624 | bytes 6161156 | tf_op jit(solution)/shard_map/dot_general | solution.py:136
  191.3 32.6 %fusion = bf16[16,2048]{1,0:T(8,128)(2,1)S(1)} fusion(bf16[192,2048]{1,0:T(8,128)(2,1)} %fusion.2), kind=kCustom, calls=%all-reduce-scatter | all-reduce-scatter fusion | flops 524289 | bytes 852480
  224.0 5.3 %collective-permute-start.15 = (bf16[16,2048]{1,0:T(8,128)(2,1)S(1)}, bf16[16,2048]{1,0:T(8,128)(2,1)S(1)}, u32[]{:S(2)}, u32[]{:S(2)}) collective-permute-start(bf16[16,2048]{1,0:T(8,128)(2,1)S(1)} %fusion), channel_id=1, source_target_pairs={{0,1},{1,2},{2,3},{3,4},{4,5},{5,6},{6,7},{7,8},{8,9},{9,10},{10,1... | collective-permute-start | bytes 196616
  229.3 7.5 %collective-permute-start.16 = (bf16[16,2048]{1,0:T(8,128)(2,1)S(1)}, bf16[16,2048]{1,0:T(8,128)(2,1)S(1)}, u32[]{:S(2)}, u32[]{:S(2)}) collective-permute-start(bf16[16,2048]{1,0:T(8,128)(2,1)S(1)} %fusion), channel_id=1, source_target_pairs={{0,2},{1,3},{2,4},{3,5},{4,6},{5,7},{6,8},{7,9},{8,10},{9,11},{10,... | collective-permute-start | bytes 196616
  236.8 7.5 %collective-permute-start.17 = (bf16[16,2048]{1,0:T(8,128)(2,1)S(1)}, bf16[16,2048]{1,0:T(8,128)(2,1)S(1)}, u32[]{:S(2)}, u32[]{:S(2)}) collective-permute-start(bf16[16,2048]{1,0:T(8,128)(2,1)S(1)} %fusion), channel_id=1, source_target_pairs={{0,3},{1,4},{2,5},{3,6},{4,7},{5,8},{6,9},{7,10},{8,11},{9,12},{10... | collective-permute-start | bytes 196616
  247.4 2.7 %collective-permute-done.18 = bf16[12,2048]{1,0:T(8,128)(2,1)S(1)} collective-permute-done((bf16[12,2048]{1,0:T(8,128)(2,1)S(1)}, bf16[12,2048]{1,0:T(8,128)(2,1)S(1)}, u32[]{:S(2)}, u32[]{:S(2)}) %collective-permute-start.18) | collective-permute-done | bytes 49184
  (150 shorter events, 53.1 us)
Async XLA Ops:
  0.6 186.7 %copy-start = (bf16[512,2048]{1,0:T(8,128)(2,1)S(1)}, bf16[512,2048]{1,0:T(8,128)(2,1)}, u32[]{:S(2)}) copy-start(bf16[512,2048]{1,0:T(8,128)(2,1)} %param.44) | copy-start | bytes 6291460
  29.8 13.3 %all-to-all-start = ((bf16[16,2,1536]{2,1,0:T(2,128)(2,1)}), bf16[16,2,1536]{2,1,0:T(2,128)(2,1)S(1)}, u32[]{:S(2)}, u32[]{:S(2)}) async-start(bf16[16,2,1536]{2,1,0:T(2,128)(2,1)} %reshape.149), calls=%async_computation | async-start | bytes 196608 | tf_op jit(solution)/shard_map/all_to_all | solution.py:94
  55.3 2.0 collective-permute-start
  57.3 3.8 %collective-permute-start.1 = (bf16[12,2048]{1,0:T(8,128)(2,1)S(1)}, bf16[12,2048]{1,0:T(8,128)(2,1)S(1)}, u32[]{:S(2)}, u32[]{:S(2)}) collective-permute-start(bf16[12,2048]{1,0:T(8,128)(2,1)S(1)} %collective-permute-done), channel_id=1, source_target_pairs={{0,1},{1,2},{2,3},{3,4},{4,5},{5,6},{6,7},{7,8},{8,9},{9,10},{10,1... | collective-permute-start | bytes 147464 | tf_op jit(solution)/shard_map/ppermute | solution.py:123
  61.1 16.4 %collective-permute-start.2 = (bf16[12,2048]{1,0:T(8,128)(2,1)S(1)}, bf16[12,2048]{1,0:T(8,128)(2,1)S(1)}, u32[]{:S(2)}, u32[]{:S(2)}) collective-permute-start(bf16[12,2048]{1,0:T(8,128)(2,1)S(1)} %collective-permute-done.1), channel_id=1, source_target_pairs={{0,1},{1,2},{2,3},{3,4},{4,5},{5,6},{6,7},{7,8},{8,9},{9,10},{10,1... | collective-permute-start | bytes 147464 | tf_op jit(solution)/shard_map/ppermute | solution.py:123
  64.2 26.5 %all-to-all-start.1 = ((bf16[16,2,2048]{2,1,0:T(2,128)(2,1)}), bf16[16,2,2048]{2,1,0:T(2,128)(2,1)S(1)}, u32[]{:S(2)}, u32[]{:S(2)}) async-start(bf16[16,2,2048]{2,1,0:T(2,128)(2,1)} %copy.88), calls=%async_computation.1 | async-start | bytes 262144 | tf_op jit(solution)/shard_map/all_to_all | solution.py:45
  77.5 3.0 %collective-permute-start.3 = (bf16[12,2048]{1,0:T(8,128)(2,1)S(1)}, bf16[12,2048]{1,0:T(8,128)(2,1)S(1)}, u32[]{:S(2)}, u32[]{:S(2)}) collective-permute-start(bf16[12,2048]{1,0:T(8,128)(2,1)S(1)} %collective-permute-done.2), channel_id=1, source_target_pairs={{0,1},{1,2},{2,3},{3,4},{4,5},{5,6},{6,7},{7,8},{8,9},{9,10},{10,1... | collective-permute-start | bytes 147464 | tf_op jit(solution)/shard_map/ppermute | solution.py:123
  80.5 4.4 %collective-permute-start.4 = (bf16[12,2048]{1,0:T(8,128)(2,1)S(1)}, bf16[12,2048]{1,0:T(8,128)(2,1)S(1)}, u32[]{:S(2)}, u32[]{:S(2)}) collective-permute-start(bf16[12,2048]{1,0:T(8,128)(2,1)S(1)} %collective-permute-done.3), channel_id=1, source_target_pairs={{0,1},{1,2},{2,3},{3,4},{4,5},{5,6},{6,7},{7,8},{8,9},{9,10},{10,1... | collective-permute-start | bytes 147464 | tf_op jit(solution)/shard_map/ppermute | solution.py:123
  84.9 4.6 %collective-permute-start.5 = (bf16[12,2048]{1,0:T(8,128)(2,1)S(1)}, bf16[12,2048]{1,0:T(8,128)(2,1)S(1)}, u32[]{:S(2)}, u32[]{:S(2)}) collective-permute-start(bf16[12,2048]{1,0:T(8,128)(2,1)S(1)} %collective-permute-done.4), channel_id=1, source_target_pairs={{0,1},{1,2},{2,3},{3,4},{4,5},{5,6},{6,7},{7,8},{8,9},{9,10},{10,1... | collective-permute-start | bytes 147464 | tf_op jit(solution)/shard_map/ppermute | solution.py:123
  89.4 4.6 %collective-permute-start.6 = (bf16[12,2048]{1,0:T(8,128)(2,1)S(1)}, bf16[12,2048]{1,0:T(8,128)(2,1)S(1)}, u32[]{:S(2)}, u32[]{:S(2)}) collective-permute-start(bf16[12,2048]{1,0:T(8,128)(2,1)S(1)} %collective-permute-done.5), channel_id=1, source_target_pairs={{0,1},{1,2},{2,3},{3,4},{4,5},{5,6},{6,7},{7,8},{8,9},{9,10},{10,1... | collective-permute-start | bytes 147464 | tf_op jit(solution)/shard_map/ppermute | solution.py:123
  94.0 4.6 %collective-permute-start.7 = (bf16[12,2048]{1,0:T(8,128)(2,1)S(1)}, bf16[12,2048]{1,0:T(8,128)(2,1)S(1)}, u32[]{:S(2)}, u32[]{:S(2)}) collective-permute-start(bf16[12,2048]{1,0:T(8,128)(2,1)S(1)} %collective-permute-done.6), channel_id=1, source_target_pairs={{0,1},{1,2},{2,3},{3,4},{4,5},{5,6},{6,7},{7,8},{8,9},{9,10},{10,1... | collective-permute-start | bytes 147464 | tf_op jit(solution)/shard_map/ppermute | solution.py:123
  98.6 5.4 %collective-permute-start.8 = (bf16[12,2048]{1,0:T(8,128)(2,1)S(1)}, bf16[12,2048]{1,0:T(8,128)(2,1)S(1)}, u32[]{:S(2)}, u32[]{:S(2)}) collective-permute-start(bf16[12,2048]{1,0:T(8,128)(2,1)S(1)} %collective-permute-done.7), channel_id=1, source_target_pairs={{0,1},{1,2},{2,3},{3,4},{4,5},{5,6},{6,7},{7,8},{8,9},{9,10},{10,1... | collective-permute-start | bytes 147464 | tf_op jit(solution)/shard_map/ppermute | solution.py:123
  104.0 20.6 %collective-permute-start.9 = (bf16[12,2048]{1,0:T(8,128)(2,1)S(1)}, bf16[12,2048]{1,0:T(8,128)(2,1)S(1)}, u32[]{:S(2)}, u32[]{:S(2)}) collective-permute-start(bf16[12,2048]{1,0:T(8,128)(2,1)S(1)} %collective-permute-done.8), channel_id=1, source_target_pairs={{0,1},{1,2},{2,3},{3,4},{4,5},{5,6},{6,7},{7,8},{8,9},{9,10},{10,1... | collective-permute-start | bytes 147464 | tf_op jit(solution)/shard_map/ppermute | solution.py:123
  107.9 33.9 %all-to-all-start.2 = ((bf16[16,2,2048]{2,1,0:T(2,128)(2,1)}), bf16[16,2,2048]{2,1,0:T(2,128)(2,1)S(1)}, u32[]{:S(2)}, u32[]{:S(2)}) async-start(bf16[16,2,2048]{2,1,0:T(2,128)(2,1)} %reshape.151), calls=%async_computation.2 | async-start | bytes 262144 | tf_op jit(solution)/shard_map/all_to_all | solution.py:47
  124.6 3.0 %collective-permute-start.10 = (bf16[12,2048]{1,0:T(8,128)(2,1)S(1)}, bf16[12,2048]{1,0:T(8,128)(2,1)S(1)}, u32[]{:S(2)}, u32[]{:S(2)}) collective-permute-start(bf16[12,2048]{1,0:T(8,128)(2,1)S(1)} %collective-permute-done.9), channel_id=1, source_target_pairs={{0,1},{1,2},{2,3},{3,4},{4,5},{5,6},{6,7},{7,8},{8,9},{9,10},{10,1... | collective-permute-start | bytes 147464 | tf_op jit(solution)/shard_map/ppermute | solution.py:123
  127.6 4.4 %collective-permute-start.11 = (bf16[12,2048]{1,0:T(8,128)(2,1)S(1)}, bf16[12,2048]{1,0:T(8,128)(2,1)S(1)}, u32[]{:S(2)}, u32[]{:S(2)}) collective-permute-start(bf16[12,2048]{1,0:T(8,128)(2,1)S(1)} %collective-permute-done.10), channel_id=1, source_target_pairs={{0,1},{1,2},{2,3},{3,4},{4,5},{5,6},{6,7},{7,8},{8,9},{9,10},{10,1... | collective-permute-start | bytes 147464 | tf_op jit(solution)/shard_map/ppermute | solution.py:123
  132.0 4.7 %collective-permute-start.12 = (bf16[12,2048]{1,0:T(8,128)(2,1)S(1)}, bf16[12,2048]{1,0:T(8,128)(2,1)}, u32[]{:S(2)}, u32[]{:S(2)}) collective-permute-start(bf16[12,2048]{1,0:T(8,128)(2,1)S(1)} %collective-permute-done.11), channel_id=1, source_target_pairs={{0,1},{1,2},{2,3},{3,4},{4,5},{5,6},{6,7},{7,8},{8,9},{9,10},{10,1... | collective-permute-start | bytes 147464 | tf_op jit(solution)/shard_map/ppermute | solution.py:123
  136.7 5.3 %collective-permute-start.13 = (bf16[12,2048]{1,0:T(8,128)(2,1)}, bf16[12,2048]{1,0:T(8,128)(2,1)}, u32[]{:S(2)}, u32[]{:S(2)}) collective-permute-start(bf16[12,2048]{1,0:T(8,128)(2,1)} %collective-permute-done.12), channel_id=1, source_target_pairs={{0,1},{1,2},{2,3},{3,4},{4,5},{5,6},{6,7},{7,8},{8,9},{9,10},{10,1... | collective-permute-start | bytes 147464 | tf_op jit(solution)/shard_map/ppermute | solution.py:123
  142.0 4.5 %collective-permute-start.14 = (bf16[12,2048]{1,0:T(8,128)(2,1)}, bf16[12,2048]{1,0:T(8,128)(2,1)}, u32[]{:S(2)}, u32[]{:S(2)}) collective-permute-start(bf16[12,2048]{1,0:T(8,128)(2,1)} %collective-permute-done.13), channel_id=1, source_target_pairs={{0,1},{1,2},{2,3},{3,4},{4,5},{5,6},{6,7},{7,8},{8,9},{9,10},{10,1... | collective-permute-start | bytes 147464 | tf_op jit(solution)/shard_map/ppermute | solution.py:123
  191.3 59.7 %copy-start.18 = (f32[12]{0:T(128)S(1)}, f32[12]{0:T(128)}, u32[]{:S(2)}) copy-start(f32[12]{0:T(128)} %copy-done.17) | copy-start | bytes 148
  224.0 26.1 %collective-permute-start.15 = (bf16[16,2048]{1,0:T(8,128)(2,1)S(1)}, bf16[16,2048]{1,0:T(8,128)(2,1)S(1)}, u32[]{:S(2)}, u32[]{:S(2)}) collective-permute-start(bf16[16,2048]{1,0:T(8,128)(2,1)S(1)} %fusion), channel_id=1, source_target_pairs={{0,1},{1,2},{2,3},{3,4},{4,5},{5,6},{6,7},{7,8},{8,9},{9,10},{10,1... | collective-permute-start | bytes 196616
  229.3 20.8 %collective-permute-start.16 = (bf16[16,2048]{1,0:T(8,128)(2,1)S(1)}, bf16[16,2048]{1,0:T(8,128)(2,1)S(1)}, u32[]{:S(2)}, u32[]{:S(2)}) collective-permute-start(bf16[16,2048]{1,0:T(8,128)(2,1)S(1)} %fusion), channel_id=1, source_target_pairs={{0,2},{1,3},{2,4},{3,5},{4,6},{5,7},{6,8},{7,9},{8,10},{9,11},{10,... | collective-permute-start | bytes 196616
  236.8 13.3 %collective-permute-start.17 = (bf16[16,2048]{1,0:T(8,128)(2,1)S(1)}, bf16[16,2048]{1,0:T(8,128)(2,1)S(1)}, u32[]{:S(2)}, u32[]{:S(2)}) collective-permute-start(bf16[16,2048]{1,0:T(8,128)(2,1)S(1)} %fusion), channel_id=1, source_target_pairs={{0,3},{1,4},{2,5},{3,6},{4,7},{5,8},{6,9},{7,10},{8,11},{9,12},{10... | collective-permute-start | bytes 196616
  244.3 5.7 %collective-permute-start.18 = (bf16[12,2048]{1,0:T(8,128)(2,1)S(1)}, bf16[12,2048]{1,0:T(8,128)(2,1)S(1)}, u32[]{:S(2)}, u32[]{:S(2)}) collective-permute-start(bf16[12,2048]{1,0:T(8,128)(2,1)S(1)} %slice.36), channel_id=1, source_target_pairs={{0,4},{1,5},{2,6},{3,7},{4,8},{5,9},{6,10},{7,11},{8,12},{9,13},{1... | collective-permute-start | bytes 147464
  (25 other events, 498.0 us)
